TPU v7x, 32 devices: a whole 2x2x4 slice. The times are simulated.
32 devices in a mesh: sp: 8 (over z, y), tp: 4 (over x, core).
Axes of the slice: x: 2, y: 2, z: 4, core: 2. Of those that a mesh axis runs over, the one named last changes fastest.
Arguments:
- resid: bfloat16 [2048, 2048], P(('sp', 'tp')), may hold values from -0.21875 to 0.21875
- query_a: bfloat16 [2048, 1024], P('sp', 'tp'), may hold values from -6 to 6
- key_a: bfloat16 [2048, 256], P('sp', 'tp'), may hold values from -6 to 6
- value_a: bfloat16 [2048, 256], P('sp', 'tp'), may hold values from -6 to 6
- query_b: bfloat16 [2048, 1024], P('sp', 'tp'), may hold values from -6 to 6
- key_b: bfloat16 [2048, 512], P('sp', 'tp'), may hold values from -6 to 6
- value_b: bfloat16 [2048, 512], P('sp', 'tp'), may hold values from -6 to 6
- gain_qa: float32 [64], replicated, may hold values from 0.1 to 8
- gain_ka: float32 [64], replicated, may hold values from 0.1 to 8
- gain_qb: float32 [128], replicated, may hold values from 0.1 to 8
- gain_kb: float32 [128], replicated, may hold values from 0.1 to 8
- w_out_a: bfloat16 [1024, 2048], P('tp'), may hold values from -0.125 to 0.125
- w_out_b: bfloat16 [1024, 2048], P('tp'), may hold values from -0.125 to 0.125
- norm_gain: float32 [2048], replicated, may hold values from 0.1 to 1.9
- w_up: bfloat16 [2048, 8192], P('sp', 'tp'), may hold values from -0.125 to 0.125
- w_down: bfloat16 [8192, 2048], P('tp', 'sp'), may hold values from -0.0625 to 0.0625
Outputs:
- result: bfloat16 [2048, 2048], P(('sp', 'tp'))
All inputs are finite; a program needn't handle non-finite values.
Results may differ from a plain program's by a relative error of at most 0.02.
The roundings to bfloat16 on the way count: a program that leaves them out, or rounds other values in their place, can miss the bound.
Values may be sent and summed in bfloat16 or wider, within the bound.
A program may use at most 128 MiB of HBM per device.

v0:
```python
import math

import jax
import jax.numpy as jnp
from jax import lax
from jax.sharding import PartitionSpec as P

GRID_W = 64


EPS = 1e-06


def norm_rope(values, gain, places):
    width = gain.shape[0]
    count = values.shape[0]
    flat = values.astype(jnp.float32).reshape(count, -1, width)
    flat = flat * lax.rsqrt(jnp.mean(flat * flat, axis=-1, keepdims=True) + EPS) * gain
    grid_rows = (places // GRID_W).astype(jnp.float32)
    grid_cols = (places % GRID_W).astype(jnp.float32)
    quarter = width // 4
    freqs = 10000.0 ** (-(2.0 * jnp.arange(quarter, dtype=jnp.float32)) / (width // 2))
    ang_r = grid_rows[:, None] * freqs
    ang_c = grid_cols[:, None] * freqs
    angles = jnp.concatenate([ang_r, ang_r, ang_c, ang_c], axis=-1)
    one, two, three, four = jnp.split(flat, 4, axis=-1)
    turned = jnp.concatenate([-two, one, -four, three], axis=-1)
    return (flat * jnp.cos(angles)[:, None, :] + turned * jnp.sin(angles)[:, None, :]).astype(
        jnp.bfloat16
    )


def fold_block(state, queries, key_block, value_block, scale):
    running, total, accum = state
    scores = (
        jnp.einsum("rkgd,pkd->kgrp", queries, key_block, preferred_element_type=jnp.float32) * scale
    )
    newest = jnp.maximum(running, jnp.max(scores, axis=-1))
    factor = jnp.exp(running - newest)
    expo = jnp.exp(scores - newest[..., None])
    total = total * factor + jnp.sum(expo, axis=-1)
    accum = accum * factor[..., None] + jnp.einsum(
        "kgrp,pkd->kgrd", expo.astype(jnp.bfloat16), value_block, preferred_element_type=jnp.float32
    )
    return (newest, total, accum)


def sweep_keys(state, queries, key_piece, value_piece, scale):
    length = key_piece.shape[0]
    block = math.gcd(length, 2048)
    blocks = length // block
    if blocks == 1:
        return fold_block(state, queries, key_piece, value_piece, scale)
    key_blocks = key_piece.reshape((blocks, block) + key_piece.shape[1:])
    value_blocks = value_piece.reshape((blocks, block) + value_piece.shape[1:])

    def advance(carry, pair):
        return (fold_block(carry, queries, pair[0], pair[1], scale), None)

    state, unused = lax.scan(advance, state, (key_blocks, value_blocks))
    return state


def start_state(queries):
    shape = (queries.shape[1], queries.shape[2], queries.shape[0])
    return (
        jnp.full(shape, -1e30, jnp.float32),
        jnp.zeros(shape, jnp.float32),
        jnp.zeros(shape + (queries.shape[3],), jnp.float32),
    )


def finish(state):
    running, total, accum = state
    outputs = accum / total[..., None]
    count = outputs.shape[2]
    return jnp.transpose(outputs, (2, 0, 1, 3)).reshape(count, -1).astype(jnp.bfloat16)


def local(
    resid,
    query_a,
    key_a,
    value_a,
    query_b,
    key_b,
    value_b,
    gain_qa,
    gain_ka,
    gain_qb,
    gain_kb,
    w_out_a,
    w_out_b,
    norm_gain,
    w_up,
    w_down,
):
    count = query_a.shape[0]
    width_a = gain_qa.shape[0]
    width_b = gain_qb.shape[0]
    places = lax.axis_index("sp") * count + jnp.arange(count, dtype=jnp.int32)
    keys_a = norm_rope(key_a, gain_ka, places)
    keys_b = norm_rope(key_b, gain_kb, places)
    heads_kv_a = keys_a.shape[1]
    heads_kv_b = keys_b.shape[1]
    queries_a = norm_rope(query_a, gain_qa, places)
    queries_b = norm_rope(query_b, gain_qb, places)
    queries_a = queries_a.reshape(count, heads_kv_a, queries_a.shape[1] // heads_kv_a, width_a)
    queries_b = queries_b.reshape(count, heads_kv_b, queries_b.shape[1] // heads_kv_b, width_b)
    values_a = value_a.reshape(count, heads_kv_a, width_a)
    values_b = value_b.reshape(count, heads_kv_b, width_b)
    state_a = sweep_keys(
        start_state(queries_a),
        queries_a,
        lax.all_gather(keys_a, "sp", axis=0, tiled=True),
        lax.all_gather(values_a, "sp", axis=0, tiled=True),
        width_a ** (-0.5),
    )
    state_b = sweep_keys(
        start_state(queries_b),
        queries_b,
        lax.all_gather(keys_b, "sp", axis=0, tiled=True),
        lax.all_gather(values_b, "sp", axis=0, tiled=True),
        width_b ** (-0.5),
    )
    attn_a = finish(state_a)
    attn_b = finish(state_b)
    rows_a, rows_b = (
        lax.all_to_all(attn_a, "tp", split_axis=0, concat_axis=1, tiled=True),
        lax.all_to_all(attn_b, "tp", split_axis=0, concat_axis=1, tiled=True),
    )
    whole_a, whole_b = (
        lax.all_gather(w_out_a, "tp", axis=0, tiled=True),
        lax.all_gather(w_out_b, "tp", axis=0, tiled=True),
    )
    proj = jnp.dot(rows_a, whole_a, preferred_element_type=jnp.float32) + jnp.dot(
        rows_b, whole_b, preferred_element_type=jnp.float32
    )
    mid = (resid.astype(jnp.float32) + proj).astype(jnp.bfloat16)
    midf = mid.astype(jnp.float32)
    normed = (
        midf * lax.rsqrt(jnp.mean(midf * midf, axis=-1, keepdims=True) + EPS) * norm_gain
    ).astype(jnp.bfloat16)
    up_whole, down_whole = (
        lax.all_gather(w_up, "sp", axis=0, tiled=True),
        lax.all_gather(w_down, "sp", axis=1, tiled=True),
    )
    hidden = jnp.square(
        jax.nn.relu(
            jnp.dot(
                lax.all_gather(normed, "tp", axis=0, tiled=True),
                up_whole,
                preferred_element_type=jnp.float32,
            )
        )
    ).astype(jnp.bfloat16)
    mixed = lax.psum_scatter(
        jnp.dot(hidden, down_whole, preferred_element_type=jnp.float32).astype(jnp.bfloat16),
        "tp",
        scatter_dimension=0,
        tiled=True,
    ).astype(jnp.float32)
    return (midf + mixed).astype(jnp.bfloat16)


def solution(mesh):
    return jax.shard_map(
        local,
        mesh=mesh,
        in_specs=(
            P(("sp", "tp"), None),
            P("sp", "tp"),
            P("sp", "tp"),
            P("sp", "tp"),
            P("sp", "tp"),
            P("sp", "tp"),
            P("sp", "tp"),
            P(),
            P(),
            P(),
            P(),
            P("tp", None),
            P("tp", None),
            P(),
            P("sp", "tp"),
            P("tp", "sp"),
        ),
        out_specs=P(("sp", "tp"), None),
        check_vma=False,
    )
```

profile of v0, /device:TPU:0, one launch (start us, length us, event | category | flops | bytes accessed | tf_op | source)
XLA Modules:
  0.0 480.9 jit_solution(12184441608509386701)
XLA Ops:
  8.1 1.0 fusion.53
  9.0 0.9 fusion.55
  10.2 1.1 reshape.505
  12.0 0.9 slice_negate_fusion.1
  13.7 33.2 %all-gather.2 = bf16[2048,128]{1,0:T(8,128)(2,1)S(1)} all-gather(bf16[256,128]{1,0:T(8,128)(2,1)S(1)} %get-tuple-element.5), channel_id=4, replica_groups=mesh['sp'=8,'tp'=4] {'sp'}, dimensions={0}, use_global_device_ids=true | all-gather | bytes 589824 | tf_op jit(solution)/shard_map/all_gather | solution.py:122
  46.9 0.9 maximum_multiply_fusion.1
  49.8 31.4 %all-gather.3 = bf16[2048,128]{1,0:T(8,128)(2,1)S(1)} all-gather(bf16[256,128]{1,0:T(8,128)(2,1)S(1)} %copy-done.5), channel_id=5, replica_groups=mesh['sp'=8,'tp'=4] {'sp'}, dimensions={0}, use_global_device_ids=true | all-gather | bytes 589824 | tf_op jit(solution)/shard_map/all_gather | solution.py:123
  81.2 0.9 fusion.31
  83.0 3.3 all-to-all-start.1
  87.2 30.7 %all-gather = bf16[2048,64]{0,1:T(8,128)(2,1)S(1)} all-gather(bf16[256,64]{0,1:T(8,128)(2,1)S(1)} %get-tuple-element.26), channel_id=2, replica_groups=mesh['sp'=8,'tp'=4] {'sp'}, dimensions={0}, use_global_device_ids=true | all-gather | bytes 294912 | tf_op jit(solution)/shard_map/all_gather | solution.py:115
  118.0 30.9 %all-gather.1 = bf16[2048,64]{0,1:T(8,128)(2,1)S(1)} all-gather(bf16[256,64]{0,1:T(8,128)(2,1)S(1)} %copy-done.6), channel_id=3, replica_groups=mesh['sp'=8,'tp'=4] {'sp'}, dimensions={0}, use_global_device_ids=true | all-gather | bytes 294912 | tf_op jit(solution)/shard_map/all_gather | solution.py:116
  148.9 1.3 bitcast_reduce_fusion
  150.2 1.4 fusion.1
  151.6 1.5 fusion.40
  154.1 3.3 all-to-all-start
  157.5 4.5 all-to-all-done
  162.1 3.0 fusion.86
  165.2 3.2 multiply_reduce_fusion
  170.5 15.7 %all-gather.14.cloned.1.call-done = bf16[256,2048]{1,0:T(8,128)(2,1)} async-done(((bf16[64,2048]{1,0:T(8,128)(2,1)}), bf16[256,2048]{1,0:T(8,128)(2,1)}) %all-gather.14.cloned.1.call-update) | async-done | bytes 1048592 | tf_op jit(solution)/shard_map/all_gather | solution.py:151
  186.2 126.5 %all-gather.16.cloned.1.call-done = bf16[2048,2048]{1,0:T(8,128)(2,1)} async-done(((bf16[256,2048]{1,0:T(8,128)(2,1)}), bf16[2048,2048]{1,0:T(8,128)(2,1)}) %all-gather.16.cloned.1.call-update) | async-done | bytes 8388624 | tf_op jit(solution)/shard_map/all_gather | solution.py:145
  312.7 125.0 %all-gather.18.cloned.1.call-done = bf16[2048,2048]{1,0:T(8,128)(2,1)} async-done(((bf16[2048,256]{1,0:T(8,128)(2,1)}), bf16[2048,2048]{1,0:T(8,128)(2,1)}) %all-gather.18.cloned.1.call-update) | async-done | bytes 8388624 | tf_op jit(solution)/shard_map/all_gather | solution.py:146
  437.7 11.5 %convolution_convert_fusion = bf16[256,2048]{1,0:T(8,128)(2,1)} fusion(bf16[2048,2048]{1,0:T(8,128)(2,1)} %all-gather.18.cloned.1.call-done, bf16[256,2048]{1,0:T(8,128)(2,1)} %all-gather.14.cloned.1.call-done, bf16[2048,2048]{1,0:T(8,128)(2,1)} %all-gather.16.cloned.1.call-done), kind=kOutput, calls=%fused_computation.15 | convolution fusion | flops 4297064448 | bytes 18874368 | tf_op jit(solution)/shard_map/dot_general | solution.py:158
  449.3 23.1 %reduce-scatter.2.cloned.1.call-done = bf16[64,2048]{1,0:T(8,128)(2,1)} async-done(((bf16[256,2048]{1,0:T(8,128)(2,1)}), bf16[64,2048]{1,0:T(8,128)(2,1)}) %reduce-scatter.2.cloned.1.call-update) | async-done | bytes 262160 | tf_op jit(solution)/shard_map/reduce_scatter | solution.py:157
  472.4 1.7 add_convert_fusion
  (81 shorter events, 9.9 us)
Async XLA Ops:
  6.5 6.5 %copy-start = (bf16[256,128]{1,0:T(8,128)(2,1)S(1)}, bf16[256,128]{1,0:T(8,128)(2,1)}, u32[]{:S(2)}) copy-start(bf16[256,128]{1,0:T(8,128)(2,1)} %param.21) | copy-start | bytes 196612
  6.5 6.5 %copy-start.8 = (f32[128]{0:T(128)S(1)}, f32[128]{0:T(128)}, u32[]{:S(2)}) copy-start(f32[128]{0:T(128)} %param.26) | copy-start | bytes 1540
  6.5 5.1 %copy-start.11 = (f32[128]{0:T(128)S(1)}, f32[128]{0:T(128)}, u32[]{:S(2)}) copy-start(f32[128]{0:T(128)} %param.25) | copy-start | bytes 1540
  6.5 155.6 %all-gather.10.cloned.1.call-start = ((), (), s32[]{:S(2)}) async-start(), calls=%async_computation.3 | async-start | bytes 5242880 | tf_op jit(solution)/shard_map/all_gather | solution.py:133
  7.3 157.9 %all-gather.12.cloned.1.call-start = ((), (), s32[]{:S(2)}) async-start(), calls=%async_computation.4 | async-start | bytes 5242880 | tf_op jit(solution)/shard_map/all_gather | solution.py:134
  10.1 38.1 %copy-start.1 = (bf16[256,256]{1,0:T(8,128)(2,1)S(1)}, bf16[256,256]{1,0:T(8,128)(2,1)}, u32[]{:S(2)}) copy-start(bf16[256,256]{1,0:T(8,128)(2,1)} %param.20) | copy-start | bytes 393220
  48.2 1.5 copy-start.5
  49.7 36.6 %copy-start.4 = (bf16[256,256]{1,0:T(8,128)(2,1)S(1)}, bf16[256,256]{1,0:T(8,128)(2,1)}, u32[]{:S(2)}) copy-start(bf16[256,256]{1,0:T(8,128)(2,1)} %param.17) | copy-start | bytes 393220
  49.7 36.7 %copy-start.10 = (f32[64]{0:T(128)S(1)}, f32[64]{0:T(128)}, u32[]{:S(2)}) copy-start(f32[64]{0:T(128)} %param.23) | copy-start | bytes 772
  49.7 36.8 %copy-start.2 = (bf16[256,64]{0,1:T(8,128)(2,1)S(1)}, bf16[256,64]{0,1:T(8,128)(2,1)}, u32[]{:S(2)}) copy-start(bf16[256,64]{0,1:T(8,128)(2,1)} %param.18) | copy-start | bytes 98308
  49.7 37.0 %copy-start.9 = (f32[64]{0:T(128)S(1)}, f32[64]{0:T(128)}, u32[]{:S(2)}) copy-start(f32[64]{0:T(128)} %param.24) | copy-start | bytes 772
  81.2 36.8 %copy-start.6 = (bf16[256,64]{0,1:T(8,128)(2,1)S(1)}, bf16[256,64]{0,1:T(8,128)(2,1)}, u32[]{:S(2)}) copy-start(bf16[256,64]{0,1:T(8,128)(2,1)} %param.19) | copy-start | bytes 98308
  83.0 71.1 %all-to-all-start.1 = ((bf16[4,64,256]{2,1,0:T(8,128)(2,1)}), bf16[4,64,256]{2,1,0:T(8,128)(2,1)S(1)}, u32[]{:S(2)}, u32[]{:S(2)}) async-start(bf16[4,64,256]{2,1,0:T(8,128)(2,1)} %convert_element_type.140), calls=%async_computation.1 | async-start | bytes 262144 | tf_op jit(solution)/shard_map/all_to_all | solution.py:130
  153.1 12.1 %copy-start.3 = (bf16[64,2048]{1,0:T(8,128)(2,1)S(1)}, bf16[64,2048]{1,0:T(8,128)(2,1)}, u32[]{:S(2)}) copy-start(bf16[64,2048]{1,0:T(8,128)(2,1)} %param.16) | copy-start | bytes 786436
  154.1 7.9 %all-to-all-start = ((bf16[4,64,256]{2,1,0:T(8,128)(2,1)}), bf16[4,64,256]{2,1,0:T(8,128)(2,1)S(1)}, u32[]{:S(2)}, u32[]{:S(2)}) async-start(bf16[4,64,256]{2,1,0:T(8,128)(2,1)} %copy.52), calls=%async_computation | async-start | bytes 262144 | tf_op jit(solution)/shard_map/all_to_all | solution.py:129
  157.5 28.7 %all-gather.14.cloned.1.call-start = ((), (), s32[]{:S(2)}) async-start(), calls=%async_computation.5 | async-start | bytes 1310720 | tf_op jit(solution)/shard_map/all_gather | solution.py:151
  162.1 6.3 %copy-start.7 = (f32[2048]{0:T(1024)S(1)}, f32[2048]{0:T(1024)}, u32[]{:S(2)}) copy-start(f32[2048]{0:T(1024)} %param.29) | copy-start | bytes 24580
  169.3 143.4 %all-gather.16.cloned.1.call-start = ((), (), s32[]{:S(2)}) async-start(), calls=%async_computation.6 | async-start | bytes 9437184 | tf_op jit(solution)/shard_map/all_gather | solution.py:145
  169.8 267.9 %all-gather.18.cloned.1.call-start = ((), (), s32[]{:S(2)}) async-start(), calls=%async_computation.7 | async-start | bytes 9437184 | tf_op jit(solution)/shard_map/all_gather | solution.py:146
  170.4 301.9 %reduce-scatter.2.cloned.1.call-start = ((), (), s32[]{:S(2)}) async-start(), calls=%async_computation.8 | async-start | bytes 1310720 | tf_op jit(solution)/shard_map/reduce_scatter | solution.py:157
Sparse Core Ops, SparseCore 0:
  8.9 37.1 all-gather.9
  47.7 34.4 all-gather.11
  169.4 16.7 all-gather.13
  188.1 124.4 all-gather.15
  314.6 123.1 all-gather.17
  449.4 22.9 reduce-scatter.1
where the time goes:
time: 481 us
  waiting for transfers between devices  297 us (62%)
  blocking collectives  126 us (26%)
  matrix products  22.3 us (5%)
  between operations  13.9 us (3%)
  other arithmetic  10.6 us (2%)
  starting transfers between devices  6.86 us (1%)
    all_gather x1, waiting for transfers between devices, local(): lax.all_gather(w_up, 'sp', axis=0, tiled=True)  126 us
    all_gather x1, waiting for transfers between devices, local(): lax.all_gather(w_down, 'sp', axis=1, tiled=True)  125 us
    all_gather x1, blocking collectives, local(): lax.all_gather(keys_b, 'sp', axis=0, tiled=True)  33.2 us
    all_gather x1, blocking collectives, local(): lax.all_gather(values_b, 'sp', axis=0, tiled=True)  31.4 us
    all_gather x1, blocking collectives, local(): lax.all_gather(values_a, 'sp', axis=0, tiled=True)  30.9 us
    all_gather x1, blocking collectives, local(): lax.all_gather(keys_a, 'sp', axis=0, tiled=True)  30.7 us
    reduce_scatter x1, waiting for transfers between devices, local(): lax.psum_scatter(jnp.dot(hidden, down_whole, preferred_element_type=jnp.f...  23.1 us
    all_gather x1, waiting for transfers between devices, local(): lax.all_gather(normed, 'tp', axis=0, tiled=True)  15.7 us
  transfers between devices with their start and end apart: 8, of which 5 were waited for; matrix products, arithmetic and copies ran while one was open for 4% of the time, Pallas kernels for 0%

commit v1 on v0

--- a/solution.py
+++ b/solution.py
@@ -3,6 +3,8 @@
 import jax
 import jax.numpy as jnp
 from jax import lax
+from jax.experimental import pallas as pl
+from jax.experimental.pallas import tpu as pltpu
 from jax.sharding import PartitionSpec as P
 
 GRID_W = 64
@@ -163,9 +165,393 @@
     return (midf + mixed).astype(jnp.bfloat16)
 
 
-def solution(mesh):
+MESH = pl.DeviceIdType.MESH
+INNER = 2
+LANES = 128
+
+
+def remote(src, dst, send, recv, target):
+    return pltpu.make_async_remote_copy(
+        src_ref=src,
+        dst_ref=dst,
+        send_sem=send,
+        recv_sem=recv,
+        device_id=target,
+        device_id_type=MESH,
+    )
+
+
+def greet(targets):
+    barrier = pltpu.get_barrier_semaphore()
+    for target in targets:
+        pl.semaphore_signal(barrier, inc=1, device_id=target, device_id_type=MESH)
+    pl.semaphore_wait(barrier, len(targets))
+
+
+def exchange_kernel(outer, kv, up, down, kv_all, up_all, down_all, send, recv, here):
+    sp = lax.axis_index("sp")
+    z = sp // INNER
+    y = sp % INNER
+    rows = up.shape[0]
+    cols = down.shape[1]
+    units = up_all.shape[1]
+    z_peers = [lax.rem(z + d, outer) for d in range(1, outer)]
+    y_peers = [lax.rem(y + d, INNER) for d in range(1, INNER)]
+    greet([{"sp": p * INNER + y} for p in z_peers] + [{"sp": z * INNER + p} for p in y_peers])
+
+    def piece(m, target):
+        at = pl.ds(pl.multiple_of(target * units, units), units)
+        if m == 0:
+            return kv
+        return up.at[:, at] if m == 1 else down.at[at, :]
+
+    def place(m, source):
+        if m == 0:
+            return kv_all.at[source]
+        if m == 1:
+            return up_all.at[pl.ds(pl.multiple_of(source * rows, rows), rows), :]
+        return down_all.at[:, pl.ds(pl.multiple_of(source * cols, cols), cols)]
+
+    started = []
+
+    def ship(m, slot, src, source, target):
+        copy = remote(src, place(m, source), send.at[m, slot], recv.at[m, source], target)
+        copy.start()
+        started.append(copy)
+
+    own = []
+    for m in range(3):
+        for i, p in enumerate(z_peers):
+            ship(m, i, piece(m, p), sp, {"sp": p * INNER + y})
+        for i, p in enumerate(y_peers):
+            ship(m, outer - 1 + i, piece(m, z), sp, {"sp": z * INNER + p})
+        copy = pltpu.make_async_copy(piece(m, z), place(m, sp), here.at[m])
+        copy.start()
+        own.append(copy)
+    for m in range(3):
+        for d in range(1, outer):
+            source = lax.rem(z + outer - d, outer) * INNER + y
+            pltpu.make_async_copy(place(m, source), place(m, source), recv.at[m, source]).wait()
+            for i, p in enumerate(y_peers):
+                ship(
+                    m,
+                    outer - 1 + d * (INNER - 1) + i,
+                    place(m, source),
+                    source,
+                    {"sp": z * INNER + p},
+                )
+    for m in range(3):
+        for p in y_peers:
+            for zs in range(outer):
+                source = zs * INNER + p
+                pltpu.make_async_copy(place(m, source), place(m, source), recv.at[m, source]).wait()
+    for copy in own:
+        copy.wait()
+    for copy in started:
+        copy.wait_send()
+
+
+def exchange(kv, up, down, total):
+    outer = total // INNER
+    units = up.shape[1] // outer
+    vmem = pl.BlockSpec(memory_space=pltpu.VMEM)
+    return pl.pallas_call(
+        lambda *refs: exchange_kernel(outer, *refs),
+        out_shape=(
+            jax.ShapeDtypeStruct((total,) + kv.shape, kv.dtype),
+            jax.ShapeDtypeStruct((up.shape[0] * total, units), up.dtype),
+            jax.ShapeDtypeStruct((units, down.shape[1] * total), down.dtype),
+        ),
+        in_specs=[vmem] * 3,
+        out_specs=(vmem,) * 3,
+        scratch_shapes=[
+            pltpu.SemaphoreType.DMA((3, total)),
+            pltpu.SemaphoreType.DMA((3, total)),
+            pltpu.SemaphoreType.DMA((3,)),
+        ],
+        compiler_params=pltpu.CompilerParams(
+            collective_id=0, has_side_effects=True, vmem_limit_bytes=40 * 1024 * 1024
+        ),
+        name="exchange",
+    )(kv, up, down)
+
+
+def tail_kernel(
+    outer,
+    sides,
+    steps,
+    part,
+    resid,
+    gain,
+    up,
+    down,
+    out,
+    part_in,
+    tokens,
+    hidden,
+    core_out,
+    core_in,
+    side_out,
+    side_in,
+    ring_out,
+    ring_in,
+    keep,
+    mid,
+    s_part,
+    r_part,
+    s_tok,
+    r_tok,
+    s_core,
+    r_core,
+    s_side,
+    r_side,
+    s_ring,
+    r_ring,
+):
+    sp = lax.axis_index("sp")
+    tp = lax.axis_index("tp")
+    z = sp // INNER
+    y = sp % INNER
+    x = tp // INNER
+    c = tp % INNER
+    lanes = sides * INNER
+    rows, width = resid.shape
+    step = width // steps
+    f32 = jnp.float32
+    z_peers = [lax.rem(z + d, outer) for d in range(1, outer)]
+    x_peers = [lax.rem(x + d, sides) for d in range(1, sides)]
+    other = 1 - c
+    tp_peers = [lax.rem(tp + d, lanes) for d in range(1, lanes)]
+    greet([{"sp": p * INNER + y} for p in z_peers] + [{"tp": p} for p in tp_peers])
+    started = []
+
+    def ship(src, dst, send, recv, target):
+        copy = remote(src, dst, send, recv, target)
+        copy.start()
+        started.append(copy)
+
+    def arrive(dst, sem):
+        pltpu.make_async_copy(dst, dst, sem).wait()
+
+    for i, p in enumerate(tp_peers):
+        ship(part.at[p], part_in.at[tp], s_part.at[i], r_part.at[tp], {"tp": p})
+    total = resid[...].astype(f32) + part[tp].astype(f32)
+    for d in range(1, lanes):
+        p = lax.rem(tp + lanes - d, lanes)
+        arrive(part_in.at[p], r_part.at[p])
+        total = total + part_in[p].astype(f32)
+    mid[...] = total.astype(jnp.bfloat16)
+    midf = mid[...].astype(f32)
+    norm = midf * lax.rsqrt(jnp.mean(midf * midf, axis=-1, keepdims=True) + EPS) * gain[...]
+    tokens[tp, z] = norm.astype(jnp.bfloat16)
+
+    sent = [0]
+
+    def pass_on(lane, zs, target):
+        ship(
+            tokens.at[lane, zs], tokens.at[lane, zs], s_tok.at[sent[0]], r_tok.at[lane, zs], target
+        )
+        sent[0] += 1
+
+    for p in z_peers:
+        pass_on(tp, z, {"sp": p * INNER + y})
+    for p in x_peers:
+        pass_on(tp, z, {"tp": p * INNER + c})
+    pass_on(tp, z, {"tp": x * INNER + other})
+    for d in range(1, outer):
+        zs = lax.rem(z + outer - d, outer)
+        arrive(tokens.at[tp, zs], r_tok.at[tp, zs])
+        for p in x_peers:
+            pass_on(tp, zs, {"tp": p * INNER + c})
+        pass_on(tp, zs, {"tp": x * INNER + other})
+
+    def feed(lane):
+        block = tokens[lane].reshape(outer * rows, width)
+        made = jnp.maximum(jnp.dot(block, up[...], preferred_element_type=f32), 0.0)
+        hidden[lane] = (made * made).astype(jnp.bfloat16)
+
+    feed(tp)
+    for d in range(1, sides):
+        lane = lax.rem(x + sides - d, sides) * INNER + c
+        for e in range(outer):
+            zs = lax.rem(z + e, outer)
+            arrive(tokens.at[lane, zs], r_tok.at[lane, zs])
+            pass_on(lane, zs, {"tp": x * INNER + other})
+        feed(lane)
+    for d in range(sides):
+        lane = lax.rem(x + d, sides) * INNER + other
+        for zs in range(outer):
+            arrive(tokens.at[lane, zs], r_tok.at[lane, zs])
+        feed(lane)
+
+    def product(lane, at):
+        return jnp.dot(hidden[lane], down[:, at], preferred_element_type=f32)
+
+    cuts = [pl.ds(j * step, step) for j in range(steps)]
+    for j, at in enumerate(cuts):
+        for d in list(range(1, sides)) + [0]:
+            side = lax.rem(x + d, sides)
+            core_out[side, :, at] = product(side * INNER + other, at).astype(jnp.bfloat16)
+            ship(
+                core_out.at[side, :, at],
+                core_in.at[side, :, at],
+                s_core.at[side, j],
+                r_core.at[side, j],
+                {"tp": x * INNER + other},
+            )
+        for d in list(range(1, sides)) + [0]:
+            side = lax.rem(x + d, sides)
+            value = product(side * INNER + c, at)
+            arrive(core_in.at[side, :, at], r_core.at[side, j])
+            value = value + core_in[side, :, at].astype(f32)
+            if d == 0:
+                keep[:, at] = value
+            else:
+                side_out[d - 1, :, at] = value.astype(jnp.bfloat16)
+                ship(
+                    side_out.at[d - 1, :, at],
+                    side_in.at[d - 1, :, at],
+                    s_side.at[d - 1, j],
+                    r_side.at[d - 1, j],
+                    {"tp": side * INNER + c},
+                )
+    for j, at in enumerate(cuts):
+        value = keep[:, at]
+        for d in range(1, sides):
+            arrive(side_in.at[d - 1, :, at], r_side.at[d - 1, j])
+            value = value + side_in[d - 1, :, at].astype(f32)
+        ring_out[:, :, at] = value.astype(jnp.bfloat16).reshape(outer, rows, step)
+        for i, p in enumerate(z_peers):
+            ship(
+                ring_out.at[p, :, at],
+                ring_in.at[i, :, at],
+                s_ring.at[i, j],
+                r_ring.at[i, j],
+                {"sp": p * INNER + y},
+            )
+    for j, at in enumerate(cuts):
+        value = mid[:, at].astype(f32) + ring_out[z, :, at].astype(f32)
+        for i in range(outer - 1):
+            arrive(ring_in.at[i, :, at], r_ring.at[i, j])
+            value = value + ring_in[i, :, at].astype(f32)
+        out[:, at] = value.astype(out.dtype)
+    for copy in started:
+        copy.wait_send()
+
+
+def tail(part, resid, gain, up, down, total, lanes):
+    outer = total // INNER
+    sides = lanes // INNER
+    rows, width = resid.shape
+    steps = 4 if width % (4 * LANES) == 0 else 1
+    units = up.shape[1]
+    band = outer * rows
+    kind = jnp.bfloat16
+    vmem = pl.BlockSpec(memory_space=pltpu.VMEM)
+    sems = pltpu.SemaphoreType.DMA
+    moves = outer - 1 + (sides - 1) * outer + outer + (sides - 1) * outer
+    near = max(sides - 1, 1)
+    return pl.pallas_call(
+        lambda *refs: tail_kernel(outer, sides, steps, *refs),
+        out_shape=jax.ShapeDtypeStruct(resid.shape, resid.dtype),
+        in_specs=[vmem] * 5,
+        out_specs=vmem,
+        scratch_shapes=[
+            pltpu.VMEM((lanes, rows, width), kind),
+            pltpu.VMEM((lanes, outer, rows, width), kind),
+            pltpu.VMEM((lanes, band, units), kind),
+            pltpu.VMEM((sides, band, width), kind),
+            pltpu.VMEM((sides, band, width), kind),
+            pltpu.VMEM((near, band, width), kind),
+            pltpu.VMEM((near, band, width), kind),
+            pltpu.VMEM((outer, rows, width), kind),
+            pltpu.VMEM((outer - 1, rows, width), kind),
+            pltpu.VMEM((band, width), jnp.float32),
+            pltpu.VMEM((rows, width), kind),
+            sems((lanes - 1,)),
+            sems((lanes,)),
+            sems((moves,)),
+            sems((lanes, outer)),
+            sems((sides, steps)),
+            sems((sides, steps)),
+            sems((near, steps)),
+            sems((near, steps)),
+            sems((outer - 1, steps)),
+            sems((outer - 1, steps)),
+        ],
+        compiler_params=pltpu.CompilerParams(
+            collective_id=1, has_side_effects=True, vmem_limit_bytes=56 * 1024 * 1024
+        ),
+        name="tail",
+    )(part, resid, gain, up, down)
+
+
+def kernel_local(
+    total,
+    lanes,
+    resid,
+    query_a,
+    key_a,
+    value_a,
+    query_b,
+    key_b,
+    value_b,
+    gain_qa,
+    gain_ka,
+    gain_qb,
+    gain_kb,
+    w_out_a,
+    w_out_b,
+    norm_gain,
+    w_up,
+    w_down,
+):
+    count = query_a.shape[0]
+    width_a = gain_qa.shape[0]
+    width_b = gain_qb.shape[0]
+    places = lax.axis_index("sp") * count + jnp.arange(count, dtype=jnp.int32)
+    keys_a = norm_rope(key_a, gain_ka, places).reshape(count, -1)
+    keys_b = norm_rope(key_b, gain_kb, places).reshape(count, -1)
+    kv = jnp.concatenate([keys_b, value_b, keys_a, value_a], axis=1)
+    kv_all, up, down = exchange(kv, w_up, w_down, total)
+    kv_all = kv_all.reshape(total * count, -1)
+    span_a = key_a.shape[1]
+    span_b = key_b.shape[1]
+    cuts = (span_b, 2 * span_b, 2 * span_b + span_a)
+    all_kb, all_vb, all_ka, all_va = jnp.split(kv_all, cuts, axis=1)
+    queries_a = norm_rope(query_a, gain_qa, places)
+    queries_b = norm_rope(query_b, gain_qb, places)
+
+    def attend(queries, keys, values, width):
+        keys = keys.reshape(keys.shape[0], -1, width)
+        values = values.reshape(values.shape[0], -1, width)
+        heads = keys.shape[1]
+        queries = queries.reshape(count, heads, queries.shape[1] // heads, width)
+        state = sweep_keys(start_state(queries), queries, keys, values, width ** (-0.5))
+        return finish(state)
+
+    attn_a = attend(queries_a, all_ka, all_va, width_a)
+    attn_b = attend(queries_b, all_kb, all_vb, width_b)
+    part = jnp.dot(attn_a, w_out_a, preferred_element_type=jnp.float32) + jnp.dot(
+        attn_b, w_out_b, preferred_element_type=jnp.float32
+    )
+    part = part.astype(jnp.bfloat16).reshape((lanes,) + resid.shape)
+    return tail(part, resid, norm_gain.reshape(1, -1), up, down, total, lanes)
+
+
+def fits(total, lanes, w_up, w_down):
+    if total % INNER or lanes % INNER or total // INNER < 2 or lanes // INNER < 2:
+        return False
+    units = w_up.shape[1] // lanes // (total // INNER)
+    rows = w_up.shape[0] // total
+    cols = w_down.shape[1] // total
+    small = 2 * units * w_up.shape[0] * 2 <= 8 * 1024 * 1024
+    return units % LANES == 0 and rows % 16 == 0 and cols % LANES == 0 and small
+
+
+def sharded(inside, mesh):
     return jax.shard_map(
-        local,
+        inside,
         mesh=mesh,
         in_specs=(
             P(("sp", "tp"), None),
@@ -188,3 +574,16 @@
         out_specs=P(("sp", "tp"), None),
         check_vma=False,
     )
+
+
+def solution(mesh):
+    total = mesh.shape["sp"]
+    lanes = mesh.shape["tp"]
+
+    def run(*args):
+        inside = local
+        if fits(total, lanes, args[-2], args[-1]):
+            inside = lambda *shards: kernel_local(total, lanes, *shards)
+        return sharded(inside, mesh)(*args)
+
+    return run

time: 481 us -> 210 us (0.44)
  waiting for transfers between devices: 297 us -> 0 us
  Pallas kernels: 0 us -> 171 us
  blocking collectives: 126 us -> 0 us
  matrix products: 22.3 us -> 6.48 us
  between operations: 13.9 us -> 0.38 us
  local copies, waits for them, and re-layouts: 3.64 us -> 13 us
  other arithmetic: 10.6 us -> 18.6 us
  starting transfers between devices: 6.86 us -> 0 us
    all_gather x5 -> x0, waiting for transfers between devices: 267 us -> none  [the longest x1 126 us: local(): lax.all_gather(w_up, 'sp', axis=0, tiled=True)]
    pallas_call x0 -> x2, Pallas kernels: none -> 171 us  [the longest x1 89.4 us: tail(): pl.pallas_call(lambda *refs: tail_kernel(outer, sides, steps, *refs), out...]
    all_gather x4 -> x0, blocking collectives: 126 us -> none  [the longest x1 33.2 us: local(): lax.all_gather(keys_b, 'sp', axis=0, tiled=True)]
    reduce_scatter x1 -> x0, waiting for transfers between devices: 23.1 us -> none  [local(): lax.psum_scatter(jnp.dot(hidden, down_whole, preferred_element_type=jnp.f...]
    dot_general x3 -> x2, matrix products: 17.8 us -> 1.9 us  [the longest x1 1.44 us: kernel_local(): jnp.dot(attn_b, w_out_b, preferred_element_type=jnp.float32)]
    all_to_all x2 -> x0, starting transfers between devices: 6.67 us -> none  [the longest x1 3.35 us: local(): lax.all_to_all(attn_a, 'tp', split_axis=0, concat_axis=1, tiled=True)]
  transfers between devices with their start and end apart: 8 -> 0, of which waited for: 5 -> 0; matrix products, arithmetic and copies ran while one was open for 4% -> 0% of each run, Pallas kernels for 0% -> 0%
where the time goes in v1:
time: 210 us
  Pallas kernels  171 us (81%)
  other arithmetic  18.6 us (9%)
  local copies, waits for them, and re-layouts  13 us (6%)
  matrix products  6.48 us (3%)
    pallas_call x1, Pallas kernels, tail(): pl.pallas_call(lambda *refs: tail_kernel(outer, sides, steps, *refs), out...  89.4 us
    pallas_call x1, Pallas kernels, exchange(): pl.pallas_call(lambda *refs: exchange_kernel(outer, *refs), out_shape=(ja...  82.1 us
    unnamed x39, local copies, waits for them, and re-layouts  4.68 us

profile of v1, /device:TPU:0, one launch (start us, length us, event | category | flops | bytes accessed | tf_op | source)
XLA Modules:
  0.0 209.9 jit_solution(17254182564517220973)
XLA Ops:
  0.0 0.9 multiply_reduce_fusion.2
  0.9 1.2 broadcast_bitcast_fusion
  2.2 0.9 fusion.39
  3.9 0.9 copy.50
  4.8 1.0 copy.52
  8.1 0.9 fusion.41
  10.0 1.0 reshape.492
  11.4 1.7 multiply_multiply_fusion
  13.1 1.0 mul.401
  15.9 1.3 fusion.44
  18.2 1.3 fusion.53
  19.6 1.0 copy.53
  20.6 1.6 copy.54
  22.2 1.1 maximum_multiply_fusion
  23.4 2.4 %slice_negate_fusion.1 = (f32[256,2,32]{2,1,0:T(2,128)S(1)}, f32[256,2,32]{2,1,0:T(2,128)S(1)}, f32[256,2,32]{2,1,0:T(2,128)S(1)}, f32[256,2,32]{2,1,0:T(2,128)S(1)}) fusion(f32[256,2,128]{2,1,0:T(2,128)} %multiply_multiply_fusion), kind=kLoop, calls=%fused_computation.36 | loop fusion | flops 32768 | bytes 524288 | tf_op jit(solution)/shard_map/neg | solution.py:29
  25.8 1.8 maximum_multiply_fusion.1
  27.6 82.1 %exchange.1 = (bf16[8,256,384]{2,1,0:T(8,128)(2,1)S(1)}, bf16[2048,512]{1,0:T(8,128)(2,1)S(1)}, bf16[512,2048]{1,0:T(8,128)(2,1)S(1)}) custom-call(bf16[256,384]{1,0:T(8,128)(2,1)S(1)} %pad_maximum_fusion.refs_0_, bf16[256,2048]{1,0:T(8,128)(2,1)S(1)} %copy-done.3, bf16[2048,256]{1,0:T(8,128)(2,1)S(1)} %copy-done.4), custom_call_target="tpu_custom_call" | custom-call | tf_op jit(solution)/shard_map/exchange/pallas_call | solution.py:258
  111.6 0.9 fusion.24
  112.5 1.2 bitcast_reduce_fusion
  113.8 1.4 fusion.1
  115.2 1.7 fusion.30
  117.4 1.4 fusion.9
  118.8 89.4 %tail.1 = bf16[64,2048]{1,0:T(8,128)(2,1)} custom-call(bf16[4,64,2048]{2,1,0:T(8,128)(2,1)} %bitcast.176, bf16[64,2048]{1,0:T(8,128)(2,1)} %refs_1_.3, f32[1,2048]{1,0:T(1,128)} %bitcast.183, bf16[2048,512]{1,0:T(8,128)(2,1)} %copy-done.1, bf16[512,2048]{1,0:T(8,128)(2,1)} %copy-done.2), custom_call_target="tpu_custom_call" | custom-call | tf_op jit(solution)/shard_map/tail/pallas_call | solution.py:454
  208.2 1.7 copy.95
  (65 shorter events, 9.7 us)
Async XLA Ops:
  0.0 116.9 %copy-start = (bf16[256,2048]{1,0:T(8,128)(2,1)S(1)}, bf16[256,2048]{1,0:T(8,128)(2,1)}, u32[]{:S(2)}) copy-start(bf16[256,2048]{1,0:T(8,128)(2,1)} %param.27) | copy-start | bytes 3145732
  0.0 15.9 %copy-start.10 = (bf16[256,128]{1,0:T(8,128)(2,1)S(1)}, bf16[256,128]{1,0:T(8,128)(2,1)}, u32[]{:S(2)}) copy-start(bf16[256,128]{1,0:T(8,128)(2,1)} %param.21) | copy-start | bytes 196612
  0.0 15.9 %copy-start.15 = (f32[128]{0:T(128)S(1)}, f32[128]{0:T(128)}, u32[]{:S(2)}) copy-start(f32[128]{0:T(128)} %param.26) | copy-start | bytes 1540
  5.8 12.4 %copy-start.16 = (f32[64]{0:T(128)S(1)}, f32[64]{0:T(128)}, u32[]{:S(2)}) copy-start(f32[64]{0:T(128)} %param.24) | copy-start | bytes 772
  6.6 0.7 copy-start.5
  11.0 7.1 %copy-start.6 = (f32[256,64]{1,0:T(8,128)S(1)}, f32[256,64]{1,0:T(8,128)}, u32[]{:S(2)}) copy-start(f32[256,64]{1,0:T(8,128)} %copy-done.5) | copy-start | bytes 196612
  11.0 7.1 %copy-start.12 = (f32[256,16]{1,0:T(8,128)S(1)}, f32[256,16]{1,0:T(8,128)}, u32[]{:S(2)}) copy-start(f32[256,16]{1,0:T(8,128)} %get-tuple-element.41) | copy-start | bytes 49156
  11.0 7.1 %copy-start.13 = (f32[256,16]{1,0:T(8,128)S(1)}, f32[256,16]{1,0:T(8,128)}, u32[]{:S(2)}) copy-start(f32[256,16]{1,0:T(8,128)} %get-tuple-element.42) | copy-start | bytes 49156
  11.0 8.5 %copy-start.14 = (bf16[256,128]{1,0:T(8,128)(2,1)S(1)}, bf16[256,128]{1,0:T(8,128)(2,1)}, u32[]{:S(2)}) copy-start(bf16[256,128]{1,0:T(8,128)(2,1)} %param.22) | copy-start | bytes 196612
  17.2 10.4 %copy-start.3 = (bf16[256,2048]{1,0:T(8,128)(2,1)S(1)}, bf16[256,2048]{1,0:T(8,128)(2,1)}, u32[]{:S(2)}) copy-start(bf16[256,2048]{1,0:T(8,128)(2,1)} %refs_1_.2) | copy-start | bytes 3145732
  17.2 10.4 %copy-start.4 = (bf16[2048,256]{1,0:T(8,128)(2,1)S(1)}, bf16[2048,256]{1,0:T(8,128)(2,1)}, u32[]{:S(2)}) copy-start(bf16[2048,256]{1,0:T(8,128)(2,1)} %refs_2_.1) | copy-start | bytes 3145732
  19.5 90.2 %copy-start.17 = (f32[256]{0:T(256)S(1)}, f32[256]{0:T(256)}, u32[]{:S(2)}) copy-start(f32[256]{0:T(256)} %broadcast_bitcast_fusion) | copy-start | bytes 3076
  22.2 87.5 %copy-start.7 = (f32[256,2,128]{2,1,0:T(2,128)S(1)}, f32[256,2,128]{2,1,0:T(2,128)}, u32[]{:S(2)}) copy-start(f32[256,2,128]{2,1,0:T(2,128)} %mul.401) | copy-start | bytes 786436
  22.2 87.5 %copy-start.8 = (f32[256,2,128]{2,1,0:T(2,128)S(1)}, f32[256,2,128]{2,1,0:T(2,128)}, u32[]{:S(2)}) copy-start(f32[256,2,128]{2,1,0:T(2,128)} %mul.408) | copy-start | bytes 786436
  22.2 87.5 %copy-start.11 = (bf16[256,256]{1,0:T(8,128)(2,1)S(1)}, bf16[256,256]{1,0:T(8,128)(2,1)}, u32[]{:S(2)}) copy-start(bf16[256,256]{1,0:T(8,128)(2,1)} %param.20) | copy-start | bytes 393220
  109.7 1.5 copy-start.1
  109.7 1.9 copy-start.2
  115.2 2.2 %copy-start.9 = (bf16[256,2048]{1,0:T(8,128)(2,1)S(1)}, bf16[256,2048]{1,0:T(8,128)(2,1)}, u32[]{:S(2)}) copy-start(bf16[256,2048]{1,0:T(8,128)(2,1)} %param.28) | copy-start | bytes 3145732

commit v2 on v0

--- a/solution.py
+++ b/solution.py
@@ -3,6 +3,8 @@
 import jax
 import jax.numpy as jnp
 from jax import lax
+from jax.experimental import pallas as pl
+from jax.experimental.pallas import tpu as pltpu
 from jax.sharding import PartitionSpec as P
 
 GRID_W = 64
@@ -163,9 +165,532 @@
     return (midf + mixed).astype(jnp.bfloat16)
 
 
-def solution(mesh):
+MESH = pl.DeviceIdType.MESH
+INNER = 2
+LANES = 128
+
+
+def remote(src, dst, send, recv, target):
+    return pltpu.make_async_remote_copy(
+        src_ref=src,
+        dst_ref=dst,
+        send_sem=send,
+        recv_sem=recv,
+        device_id=target,
+        device_id_type=MESH,
+    )
+
+
+def greet(targets):
+    barrier = pltpu.get_barrier_semaphore()
+    for target in targets:
+        pl.semaphore_signal(barrier, inc=1, device_id=target, device_id_type=MESH)
+    pl.semaphore_wait(barrier, len(targets))
+
+
+def flip(place, k):
+    bit = 1
+    while bit <= k:
+        if k & bit:
+            place = place + bit - 2 * bit * lax.rem(place // bit, 2)
+        bit *= 2
+    return place
+
+
+def peers_of(place, count):
+    return [flip(place, k) for k in range(count - 1, 0, -1)]
+
+
+def arrive(dst, sem):
+    pltpu.make_async_copy(dst, dst, sem).wait()
+
+
+def front_kernel(
+    outer,
+    lanes,
+    scales,
+    kv_in,
+    q_a,
+    q_b,
+    table,
+    gains,
+    resid,
+    norm_gain,
+    out_a,
+    out_b,
+    up,
+    down,
+    up_all,
+    down_all,
+    mid,
+    normed,
+    kv,
+    kv_all,
+    attn,
+    part,
+    part_in,
+    send,
+    recv,
+    here,
+    s_part,
+    r_part,
+):
+    f32 = jnp.float32
+    sp = lax.axis_index("sp")
+    tp = lax.axis_index("tp")
+    z = sp // INNER
+    y = sp % INNER
+    rows = up.shape[0]
+    cols = down.shape[1]
+    units = up_all.shape[1]
+    count = q_a.shape[0]
+    total = outer * INNER
+    z_peers = peers_of(z, outer)
+    y_peers = peers_of(y, INNER)
+    tp_peers = peers_of(tp, lanes)
+    greet(
+        [{"sp": p * INNER + y} for p in z_peers]
+        + [{"sp": z * INNER + p} for p in y_peers]
+        + [{"tp": p} for p in tp_peers]
+    )
+    lane = lax.broadcasted_iota(jnp.int32, (count, LANES), 1)
+    low = lane < LANES // 2
+
+    def spin(value, quarter):
+        even = lax.rem(lane // quarter, 2) == 0
+        ahead = pltpu.roll(value, LANES - quarter, 1)
+        behind = pltpu.roll(value, quarter, 1)
+        return jnp.where(even, -ahead, behind)
+
+    def turn_b(raw, gain):
+        value = raw.astype(f32)
+        value = value * lax.rsqrt(jnp.mean(value * value, axis=-1, keepdims=True) + EPS) * gain
+        return value * table[:, 0:LANES] + spin(value, LANES // 4) * table[:, LANES : 2 * LANES]
+
+    def turn_a(raw, gain):
+        value = raw.astype(f32)
+        square = value * value
+        first = jnp.sum(jnp.where(low, square, 0.0), axis=-1, keepdims=True)
+        second = jnp.sum(jnp.where(low, 0.0, square), axis=-1, keepdims=True)
+        mean = jnp.where(low, first, second) * (2.0 / LANES)
+        value = value * lax.rsqrt(mean + EPS) * gain
+        cosine = table[:, 2 * LANES : 3 * LANES]
+        sine = table[:, 3 * LANES : 4 * LANES]
+        return value * cosine + spin(value, LANES // 8) * sine
+
+    raw = kv_in[:, 2 * LANES : 3 * LANES]
+    keys = turn_a(raw, gains[3:4, :])
+    kv[:, 2 * LANES : 3 * LANES] = jnp.where(low, keys, raw.astype(f32)).astype(jnp.bfloat16)
+    kv[:, 0:LANES] = turn_b(kv_in[:, 0:LANES], gains[1:2, :]).astype(jnp.bfloat16)
+    kv[:, LANES : 2 * LANES] = kv_in[:, LANES : 2 * LANES]
+
+    def piece(m, target):
+        at = pl.ds(pl.multiple_of(target * units, units), units)
+        if m == 0:
+            return kv
+        return up.at[:, at] if m == 1 else down.at[at, :]
+
+    def place(m, source):
+        if m == 0:
+            return kv_all.at[source]
+        if m == 1:
+            return up_all.at[pl.ds(pl.multiple_of(source * rows, rows), rows), :]
+        return down_all.at[:, pl.ds(pl.multiple_of(source * cols, cols), cols)]
+
+    started = []
+
+    def ship(m, slot, src, source, target):
+        copy = remote(src, place(m, source), send.at[m, slot], recv.at[m, source], target)
+        copy.start()
+        started.append(copy)
+
+    def open_z(m):
+        for i, p in enumerate(z_peers):
+            ship(m, i, piece(m, p), sp, {"sp": p * INNER + y})
+
+    def open_y(m):
+        for i, p in enumerate(y_peers):
+            ship(m, outer - 1 + i, piece(m, z), sp, {"sp": z * INNER + p})
+
+    def forward(m, i):
+        source = z_peers[i] * INNER + y
+        arrive(place(m, source), recv.at[m, source])
+        for n, p in enumerate(y_peers):
+            slot = outer - 1 + (i + 1) * (INNER - 1) + n
+            ship(m, slot, place(m, source), source, {"sp": z * INNER + p})
+
+    def settle(m):
+        for p in y_peers:
+            for zs in range(outer):
+                source = zs * INNER + p
+                arrive(place(m, source), recv.at[m, source])
+
+    own = []
+    open_z(0)
+    open_y(0)
+    for m in (1, 2):
+        open_z(m)
+    open_y(1)
+    for m in range(3):
+        copy = pltpu.make_async_copy(piece(m, z), place(m, sp), here.at[m])
+        copy.start()
+        own.append(copy)
+    wide = q_a.shape[1] // LANES
+    tall = q_b.shape[1] // LANES
+    turned_a = []
+    turned_b = []
+    for n in range(wide):
+        value = turn_a(q_a[:, n * LANES : (n + 1) * LANES], gains[2:3, :])
+        other = pltpu.roll(value, LANES // 2, 1)
+        for v in (value, other):
+            turned_a.append(jnp.where(low, v, 0.0).astype(jnp.bfloat16))
+    for n in range(tall):
+        value = turn_b(q_b[:, n * LANES : (n + 1) * LANES], gains[0:1, :])
+        turned_b.append(value.astype(jnp.bfloat16))
+    for i in range(outer - 1):
+        forward(0, i)
+    open_y(2)
+    own[0].wait()
+    settle(0)
+
+    def attend(query, keys, values, scale):
+        scores = lax.dot_general(
+            query, keys, (((1,), (1,)), ((), ())), preferred_element_type=f32
+        )
+        scores = scores * scale
+        expo = jnp.exp(scores - jnp.max(scores, axis=-1, keepdims=True))
+        summed = jnp.dot(expo.astype(jnp.bfloat16), values, preferred_element_type=f32)
+        return summed / jnp.sum(expo, axis=-1, keepdims=True)
+
+    both = kv_all[:, :, 2 * LANES : 3 * LANES].reshape(total * count, LANES)
+    for n in range(wide):
+        first = attend(turned_a[2 * n], both, both, scales[0])
+        second = attend(turned_a[2 * n + 1], both, both, scales[0])
+        pair = jnp.where(low, pltpu.roll(first, LANES // 2, 1), second)
+        attn[:, n * LANES : (n + 1) * LANES] = pair.astype(jnp.bfloat16)
+    forward(1, 0)
+    keys = kv_all[:, :, 0:LANES].reshape(total * count, LANES)
+    values = kv_all[:, :, LANES : 2 * LANES].reshape(total * count, LANES)
+    for n in range(tall):
+        made = attend(turned_b[n], keys, values, scales[1])
+        attn[:, (wide + n) * LANES : (wide + n + 1) * LANES] = made.astype(jnp.bfloat16)
+    split = wide * LANES
+    band = resid.shape[0]
+    for p in tp_peers + [tp]:
+        at = pl.ds(pl.multiple_of(p * band, band), band)
+        part[p] = (
+            jnp.dot(attn[at, 0:split], out_a[...], preferred_element_type=f32)
+            + jnp.dot(attn[at, split:], out_b[...], preferred_element_type=f32)
+        ).astype(jnp.bfloat16)
+    for i, p in enumerate(tp_peers):
+        copy = remote(part.at[p], part_in.at[tp], s_part.at[i], r_part.at[tp], {"tp": p})
+        copy.start()
+        started.append(copy)
+    for i in range(1, outer - 1):
+        forward(1, i)
+    sums = resid[...].astype(f32) + part[tp].astype(f32)
+    for p in tp_peers:
+        arrive(part_in.at[p], r_part.at[p])
+        sums = sums + part_in[p].astype(f32)
+    mid[...] = sums.astype(jnp.bfloat16)
+    midf = mid[...].astype(f32)
+    norm = lax.rsqrt(jnp.mean(midf * midf, axis=-1, keepdims=True) + EPS)
+    normed[...] = (midf * norm * norm_gain[...]).astype(jnp.bfloat16)
+    for i in range(outer - 1):
+        forward(2, i)
+    settle(1)
+    settle(2)
+    for copy in own[1:]:
+        copy.wait()
+    for copy in started:
+        copy.wait_send()
+
+
+def front(kv, q_a, q_b, table, gains, resid, norm_gain, out_a, out_b, up, down, total, lanes):
+    outer = total // INNER
+    units = up.shape[1] // outer
+    kind = jnp.bfloat16
+    scales = ((LANES // 2) ** (-0.5), LANES ** (-0.5))
+    features = q_a.shape[1] + q_b.shape[1]
+    vmem = pl.BlockSpec(memory_space=pltpu.VMEM)
+    sems = pltpu.SemaphoreType.DMA
+    return pl.pallas_call(
+        lambda *refs: front_kernel(outer, lanes, scales, *refs),
+        out_shape=(
+            jax.ShapeDtypeStruct((up.shape[0] * total, units), up.dtype),
+            jax.ShapeDtypeStruct((units, down.shape[1] * total), down.dtype),
+            jax.ShapeDtypeStruct(resid.shape, resid.dtype),
+            jax.ShapeDtypeStruct(resid.shape, resid.dtype),
+        ),
+        in_specs=[vmem] * 11,
+        out_specs=(vmem,) * 4,
+        scratch_shapes=[
+            pltpu.VMEM(kv.shape, kind),
+            pltpu.VMEM((total,) + kv.shape, kind),
+            pltpu.VMEM((q_a.shape[0], features), kind),
+            pltpu.VMEM((lanes,) + resid.shape, kind),
+            pltpu.VMEM((lanes,) + resid.shape, kind),
+            sems((3, total)),
+            sems((3, total)),
+            sems((3,)),
+            sems((lanes - 1,)),
+            sems((lanes,)),
+        ],
+        compiler_params=pltpu.CompilerParams(
+            collective_id=0, has_side_effects=True, vmem_limit_bytes=56 * 1024 * 1024
+        ),
+        name="front",
+    )(kv, q_a, q_b, table, gains, resid, norm_gain, out_a, out_b, up, down)
+
+
+def tail_kernel(
+    outer,
+    sides,
+    normed,
+    mid,
+    up,
+    down,
+    out,
+    tokens,
+    core_out,
+    core_in,
+    side_out,
+    side_in,
+    keep,
+    ring_out,
+    ring_in,
+    s_tok,
+    r_tok,
+    s_core,
+    r_core,
+    s_side,
+    r_side,
+    s_ring,
+    r_ring,
+):
+    sp = lax.axis_index("sp")
+    tp = lax.axis_index("tp")
+    z = sp // INNER
+    y = sp % INNER
+    x = tp // INNER
+    c = tp % INNER
+    lanes = sides * INNER
+    rows, width = mid.shape
+    f32 = jnp.float32
+    z_peers = peers_of(z, outer)
+    x_peers = peers_of(x, sides)
+    other = 1 - c
+    greet(
+        [{"sp": p * INNER + y} for p in z_peers]
+        + [{"tp": p * INNER + c} for p in x_peers]
+        + [{"tp": x * INNER + other}]
+    )
+    started = []
+
+    def ship(src, dst, send, recv, target):
+        copy = remote(src, dst, send, recv, target)
+        copy.start()
+        started.append(copy)
+
+    sent = [0]
+
+    def pass_on(src, k, lane, target):
+        ship(src, tokens.at[k, lane], s_tok.at[sent[0]], r_tok.at[k, lane], target)
+        sent[0] += 1
+
+    for k, p in enumerate(z_peers):
+        pass_on(normed, k + 1, tp, {"sp": p * INNER + y})
+    for p in x_peers:
+        pass_on(normed, 0, tp, {"tp": p * INNER + c})
+    pass_on(normed, 0, tp, {"tp": x * INNER + other})
+    tokens[0, tp] = normed[...]
+
+    def spread(k):
+        arrive(tokens.at[k, tp], r_tok.at[k, tp])
+        for p in x_peers:
+            pass_on(tokens.at[k, tp], k, tp, {"tp": p * INNER + c})
+        pass_on(tokens.at[k, tp], k, tp, {"tp": x * INNER + other})
+
+    def relay(k):
+        for p in x_peers:
+            lane = p * INNER + c
+            arrive(tokens.at[k, lane], r_tok.at[k, lane])
+            pass_on(tokens.at[k, lane], k, lane, {"tp": x * INNER + other})
+
+    def complete(k):
+        value = keep[k]
+        for d in range(sides - 1):
+            arrive(side_in.at[k, d], r_side.at[k, d])
+            value = value + side_in[k, d].astype(f32)
+        if k == 0:
+            keep[0] = value
+            return
+        ring_out[k - 1] = value.astype(jnp.bfloat16)
+        target = {"sp": z_peers[k - 1] * INNER + y}
+        ship(ring_out.at[k - 1], ring_in.at[k - 1], s_ring.at[k - 1], r_ring.at[k - 1], target)
+
+    for k in range(outer):
+        relay(k)
+        if k + 1 < outer:
+            spread(k + 1)
+        for p in range(sides):
+            lane = p * INNER + other
+            arrive(tokens.at[k, lane], r_tok.at[k, lane])
+        block = tokens[k].reshape(lanes * rows, width)
+        made = jnp.maximum(jnp.dot(block, up[...], preferred_element_type=f32), 0.0)
+        hidden = (made * made).astype(jnp.bfloat16)
+        sums = jnp.dot(hidden, down[...], preferred_element_type=f32)
+        sums = sums.reshape(sides, INNER, rows, width)
+        mine = jnp.where(c == 0, sums[:, 0], sums[:, 1])
+        core_out[k] = jnp.where(c == 0, sums[:, 1], sums[:, 0]).astype(jnp.bfloat16)
+        ship(core_out.at[k], core_in.at[k], s_core.at[k], r_core.at[k], {"tp": x * INNER + other})
+        if k >= 1:
+            complete(k - 1)
+        arrive(core_in.at[k], r_core.at[k])
+        mine = mine + core_in[k].astype(f32)
+        side_out[k] = mine.astype(jnp.bfloat16)
+        held = mine[0]
+        for n in range(1, sides):
+            held = jnp.where(x == n, mine[n], held)
+        keep[k] = held
+        for d, p in enumerate(x_peers):
+            ship(
+                side_out.at[k, p],
+                side_in.at[k, d],
+                s_side.at[k, d],
+                r_side.at[k, d],
+                {"tp": p * INNER + c},
+            )
+    complete(outer - 1)
+    value = mid[...].astype(f32) + keep[0]
+    for k in range(outer - 1):
+        arrive(ring_in.at[k], r_ring.at[k])
+        value = value + ring_in[k].astype(f32)
+    out[...] = value.astype(out.dtype)
+    for copy in started:
+        copy.wait_send()
+
+
+def tail(normed, mid, up, down, total, lanes):
+    outer = total // INNER
+    sides = lanes // INNER
+    rows, width = mid.shape
+    kind = jnp.bfloat16
+    vmem = pl.BlockSpec(memory_space=pltpu.VMEM)
+    sems = pltpu.SemaphoreType.DMA
+    moves = outer - 1 + outer * (2 * sides - 1)
+    near = sides - 1
+    far = outer - 1
+    return pl.pallas_call(
+        lambda *refs: tail_kernel(outer, sides, *refs),
+        out_shape=jax.ShapeDtypeStruct(mid.shape, mid.dtype),
+        in_specs=[vmem] * 4,
+        out_specs=vmem,
+        scratch_shapes=[
+            pltpu.VMEM((outer, lanes, rows, width), kind),
+            pltpu.VMEM((outer, sides, rows, width), kind),
+            pltpu.VMEM((outer, sides, rows, width), kind),
+            pltpu.VMEM((outer, sides, rows, width), kind),
+            pltpu.VMEM((outer, near, rows, width), kind),
+            pltpu.VMEM((outer, rows, width), jnp.float32),
+            pltpu.VMEM((far, rows, width), kind),
+            pltpu.VMEM((far, rows, width), kind),
+            sems((moves,)),
+            sems((outer, lanes)),
+            sems((outer,)),
+            sems((outer,)),
+            sems((outer, near)),
+            sems((outer, near)),
+            sems((far,)),
+            sems((far,)),
+        ],
+        compiler_params=pltpu.CompilerParams(
+            collective_id=1, has_side_effects=True, vmem_limit_bytes=56 * 1024 * 1024
+        ),
+        name="tail",
+    )(normed, mid, up, down)
+
+
+def turning_table(places, width, repeat):
+    quarter = width // 4
+    index = jnp.arange(width * repeat, dtype=jnp.int32) % width
+    freqs = 10000.0 ** (-(2.0 * (index % quarter).astype(jnp.float32)) / (width // 2))
+    grid = jnp.where(index < width // 2, places[:, None] // GRID_W, places[:, None] % GRID_W)
+    angles = grid.astype(jnp.float32) * freqs
+    return [jnp.cos(angles), jnp.sin(angles)]
+
+
+def kernel_local(
+    total,
+    lanes,
+    resid,
+    query_a,
+    key_a,
+    value_a,
+    query_b,
+    key_b,
+    value_b,
+    gain_qa,
+    gain_ka,
+    gain_qb,
+    gain_kb,
+    w_out_a,
+    w_out_b,
+    norm_gain,
+    w_up,
+    w_down,
+):
+    count = query_a.shape[0]
+    places = lax.axis_index("sp") * count + jnp.arange(count, dtype=jnp.int32)
+    kv = jnp.concatenate([key_b, value_b, key_a, value_a], axis=1)
+    table = jnp.concatenate(
+        turning_table(places, gain_qb.shape[0], 1) + turning_table(places, gain_qa.shape[0], 2),
+        axis=1,
+    )
+    gains = jnp.stack([gain_qb, gain_kb, jnp.tile(gain_qa, 2), jnp.tile(gain_ka, 2)])
+    up, down, mid, normed = front(
+        kv,
+        query_a,
+        query_b,
+        table,
+        gains,
+        resid,
+        norm_gain.reshape(1, -1),
+        w_out_a,
+        w_out_b,
+        w_up,
+        w_down,
+        total,
+        lanes,
+    )
+    return tail(normed, mid, up, down, total, lanes)
+
+
+def fits(total, lanes, args):
+    outer = total // INNER
+    sides = lanes // INNER
+    if total % INNER or lanes % INNER or outer < 2 or sides < 2:
+        return False
+    if outer & (outer - 1) or sides & (sides - 1):
+        return False
+    key_a, key_b, gain_a, gain_b = args[2], args[5], args[7], args[9]
+    if 2 * gain_a.shape[0] != LANES or gain_b.shape[0] != LANES:
+        return False
+    if key_a.shape[1] != lanes * LANES // 2 or key_b.shape[1] != lanes * LANES:
+        return False
+    if args[1].shape[1] % (lanes * LANES) or args[4].shape[1] % (lanes * LANES):
+        return False
+    w_up, w_down = args[-2], args[-1]
+    units = w_up.shape[1] // lanes // outer
+    rows = w_up.shape[0] // total
+    cols = w_down.shape[1] // total
+    small = units * w_up.shape[0] <= 2**20 and args[0].shape[0] <= 2**11
+    return units % LANES == 0 and rows % 16 == 0 and cols % LANES == 0 and small
+
+
+def sharded(inside, mesh):
     return jax.shard_map(
-        local,
+        inside,
         mesh=mesh,
         in_specs=(
             P(("sp", "tp"), None),
@@ -188,3 +713,16 @@
         out_specs=P(("sp", "tp"), None),
         check_vma=False,
     )
+
+
+def solution(mesh):
+    total = mesh.shape["sp"]
+    lanes = mesh.shape["tp"]
+
+    def run(*args):
+        inside = local
+        if fits(total, lanes, args):
+            inside = lambda *shards: kernel_local(total, lanes, *shards)
+        return sharded(inside, mesh)(*args)
+
+    return run

time: 481 us -> 174 us (0.36)
  waiting for transfers between devices: 297 us -> 0 us
  Pallas kernels: 0 us -> 164 us
  blocking collectives: 126 us -> 0 us
  matrix products: 22.3 us -> 0 us
  between operations: 13.9 us -> 0.04 us
  starting transfers between devices: 6.86 us -> 0 us
  other arithmetic: 10.6 us -> 4.79 us
    all_gather x5 -> x0, waiting for transfers between devices: 267 us -> none  [the longest x1 126 us: local(): lax.all_gather(w_up, 'sp', axis=0, tiled=True)]
    pallas_call x0 -> x2, Pallas kernels: none -> 164 us  [the longest x1 92.8 us: front(): pl.pallas_call(lambda *refs: front_kernel(outer, lanes, scales, *refs), o...]
    all_gather x4 -> x0, blocking collectives: 126 us -> none  [the longest x1 33.2 us: local(): lax.all_gather(keys_b, 'sp', axis=0, tiled=True)]
    reduce_scatter x1 -> x0, waiting for transfers between devices: 23.1 us -> none  [local(): lax.psum_scatter(jnp.dot(hidden, down_whole, preferred_element_type=jnp.f...]
    dot_general x7 -> x0, matrix products: 22.3 us -> none  [the longest x1 11.5 us: local(): jnp.dot(hidden, down_whole, preferred_element_type=jnp.float32)]
    all_to_all x2 -> x0, starting transfers between devices: 6.67 us -> none  [the longest x1 3.35 us: local(): lax.all_to_all(attn_a, 'tp', split_axis=0, concat_axis=1, tiled=True)]
  transfers between devices with their start and end apart: 8 -> 0, of which waited for: 5 -> 0; matrix products, arithmetic and copies ran while one was open for 4% -> 0% of each run, Pallas kernels for 0% -> 0%
where the time goes in v2:
time: 174 us; the launch traced here: 173 us
  Pallas kernels  164 us (94%)
  local copies, waits for them, and re-layouts  4.9 us (3%)
  other arithmetic  4.79 us (3%)
    pallas_call x1, Pallas kernels, front(): pl.pallas_call(lambda *refs: front_kernel(outer, lanes, scales, *refs), o...  92.8 us
    pallas_call x1, Pallas kernels, tail(): pl.pallas_call(lambda *refs: tail_kernel(outer, sides, *refs), out_shape=...  70.9 us

profile of v2, /device:TPU:0, one launch (start us, length us, event | category | flops | bytes accessed | tf_op | source)
XLA Modules:
  0.0 173.5 jit_solution(4946679829512975645)
XLA Ops:
  0.0 0.7 tile.4
  0.7 0.1 stack_tile.6
  0.7 0.7 tile.5
  1.4 0.1 stack_tile.7
  1.5 1.3 pad_maximum_fusion.2.refs_4_
  2.8 0.9 copy.17
  3.6 0.9 copy.18
  4.5 1.6 pad_maximum_fusion.1.refs_0_
  6.2 1.0 fusion.3
  7.2 0.9 pad_maximum_fusion.refs_3_
  8.0 92.8 %front.1 = (bf16[2048,512]{1,0:T(8,128)(2,1)}, bf16[512,2048]{1,0:T(8,128)(2,1)}, bf16[64,2048]{1,0:T(8,128)(2,1)}, bf16[64,2048]{1,0:T(8,128)(2,1)}) custom-call(bf16[256,384]{1,0:T(8,128)(2,1)} %pad_maximum_fusion.1.refs_0_, bf16[256,256]{1,0:T(8,128)(2,1)} %refs_1_.1, bf16[256,256]{1,0:T(8,128)(2,1)} %refs_2_.1, f32[256,512]{1,0:T(8,128)} %pad_maximum_fusion.refs_3_, ...), custom_call_target="tpu_custom_call" | custom-call | tf_op jit(solution)/shard_map/front/pallas_call | solution.py:417
  100.8 70.9 %tail.1 = bf16[64,2048]{1,0:T(8,128)(2,1)} custom-call(bf16[64,2048]{1,0:T(8,128)(2,1)} %get-tuple-element.9.refs_0_, bf16[64,2048]{1,0:T(8,128)(2,1)} %get-tuple-element.10.refs_1_, bf16[2048,512]{1,0:T(8,128)(2,1)} %get-tuple-element.11.refs_2_, bf16[512,2048]{1,0:T(8,128)(2,1)} %get-tuple-element.12.refs_3_), custom_call_target="tpu_custom_call" | custom-call | tf_op jit(solution)/shard_map/tail/pallas_call | solution.py:584
  171.8 1.7 copy.20
  (3 shorter events, 0.0 us)

commit v3 on v2

--- a/solution.py
+++ b/solution.py
@@ -209,11 +209,20 @@
     outer,
     lanes,
     scales,
-    kv_in,
+    k_a,
+    v_a,
+    k_b,
+    v_b,
     q_a,
     q_b,
-    table,
-    gains,
+    cos_a,
+    sin_a,
+    cos_b,
+    sin_b,
+    gain_qa,
+    gain_ka,
+    gain_qb,
+    gain_kb,
     resid,
     norm_gain,
     out_a,
@@ -265,7 +274,7 @@
     def turn_b(raw, gain):
         value = raw.astype(f32)
         value = value * lax.rsqrt(jnp.mean(value * value, axis=-1, keepdims=True) + EPS) * gain
-        return value * table[:, 0:LANES] + spin(value, LANES // 4) * table[:, LANES : 2 * LANES]
+        return value * cos_b[...] + spin(value, LANES // 4) * sin_b[...]
 
     def turn_a(raw, gain):
         value = raw.astype(f32)
@@ -274,15 +283,16 @@
         second = jnp.sum(jnp.where(low, 0.0, square), axis=-1, keepdims=True)
         mean = jnp.where(low, first, second) * (2.0 / LANES)
         value = value * lax.rsqrt(mean + EPS) * gain
-        cosine = table[:, 2 * LANES : 3 * LANES]
-        sine = table[:, 3 * LANES : 4 * LANES]
-        return value * cosine + spin(value, LANES // 8) * sine
-
-    raw = kv_in[:, 2 * LANES : 3 * LANES]
-    keys = turn_a(raw, gains[3:4, :])
-    kv[:, 2 * LANES : 3 * LANES] = jnp.where(low, keys, raw.astype(f32)).astype(jnp.bfloat16)
-    kv[:, 0:LANES] = turn_b(kv_in[:, 0:LANES], gains[1:2, :]).astype(jnp.bfloat16)
-    kv[:, LANES : 2 * LANES] = kv_in[:, LANES : 2 * LANES]
+        return value * cos_a[...] + spin(value, LANES // 8) * sin_a[...]
+
+    def twice(ref):
+        return jnp.concatenate([ref[...], ref[...]], axis=1)
+
+    raw = jnp.concatenate([k_a[...].astype(f32), v_a[...].astype(f32)], axis=1)
+    keys = turn_a(raw, twice(gain_ka))
+    kv[:, 2 * LANES : 3 * LANES] = jnp.where(low, keys, raw).astype(jnp.bfloat16)
+    kv[:, 0:LANES] = turn_b(k_b[...], gain_kb[...]).astype(jnp.bfloat16)
+    kv[:, LANES : 2 * LANES] = v_b[...]
 
     def piece(m, target):
         at = pl.ds(pl.multiple_of(target * units, units), units)
@@ -340,12 +350,12 @@
     turned_a = []
     turned_b = []
     for n in range(wide):
-        value = turn_a(q_a[:, n * LANES : (n + 1) * LANES], gains[2:3, :])
+        value = turn_a(q_a[:, n * LANES : (n + 1) * LANES], twice(gain_qa))
         other = pltpu.roll(value, LANES // 2, 1)
         for v in (value, other):
             turned_a.append(jnp.where(low, v, 0.0).astype(jnp.bfloat16))
     for n in range(tall):
-        value = turn_b(q_b[:, n * LANES : (n + 1) * LANES], gains[0:1, :])
+        value = turn_b(q_b[:, n * LANES : (n + 1) * LANES], gain_qb[...])
         turned_b.append(value.astype(jnp.bfloat16))
     for i in range(outer - 1):
         forward(0, i)
@@ -396,56 +406,23 @@
     midf = mid[...].astype(f32)
     norm = lax.rsqrt(jnp.mean(midf * midf, axis=-1, keepdims=True) + EPS)
     normed[...] = (midf * norm * norm_gain[...]).astype(jnp.bfloat16)
-    for i in range(outer - 1):
-        forward(2, i)
-    settle(1)
-    settle(2)
-    for copy in own[1:]:
-        copy.wait()
-    for copy in started:
-        copy.wait_send()
-
-
-def front(kv, q_a, q_b, table, gains, resid, norm_gain, out_a, out_b, up, down, total, lanes):
-    outer = total // INNER
-    units = up.shape[1] // outer
-    kind = jnp.bfloat16
-    scales = ((LANES // 2) ** (-0.5), LANES ** (-0.5))
-    features = q_a.shape[1] + q_b.shape[1]
-    vmem = pl.BlockSpec(memory_space=pltpu.VMEM)
-    sems = pltpu.SemaphoreType.DMA
-    return pl.pallas_call(
-        lambda *refs: front_kernel(outer, lanes, scales, *refs),
-        out_shape=(
-            jax.ShapeDtypeStruct((up.shape[0] * total, units), up.dtype),
-            jax.ShapeDtypeStruct((units, down.shape[1] * total), down.dtype),
-            jax.ShapeDtypeStruct(resid.shape, resid.dtype),
-            jax.ShapeDtypeStruct(resid.shape, resid.dtype),
-        ),
-        in_specs=[vmem] * 11,
-        out_specs=(vmem,) * 4,
-        scratch_shapes=[
-            pltpu.VMEM(kv.shape, kind),
-            pltpu.VMEM((total,) + kv.shape, kind),
-            pltpu.VMEM((q_a.shape[0], features), kind),
-            pltpu.VMEM((lanes,) + resid.shape, kind),
-            pltpu.VMEM((lanes,) + resid.shape, kind),
-            sems((3, total)),
-            sems((3, total)),
-            sems((3,)),
-            sems((lanes - 1,)),
-            sems((lanes,)),
-        ],
-        compiler_params=pltpu.CompilerParams(
-            collective_id=0, has_side_effects=True, vmem_limit_bytes=56 * 1024 * 1024
-        ),
-        name="front",
-    )(kv, q_a, q_b, table, gains, resid, norm_gain, out_a, out_b, up, down)
+    forward(2, 0)
+
+    def close():
+        for i in range(1, outer - 1):
+            forward(2, i)
+        settle(1)
+        settle(2)
+        for copy in own[1:]:
+            copy.wait()
+
+    return close, started
 
 
 def tail_kernel(
     outer,
     sides,
+    close,
     normed,
     mid,
     up,
@@ -480,11 +457,6 @@
     z_peers = peers_of(z, outer)
     x_peers = peers_of(x, sides)
     other = 1 - c
-    greet(
-        [{"sp": p * INNER + y} for p in z_peers]
-        + [{"tp": p * INNER + c} for p in x_peers]
-        + [{"tp": x * INNER + other}]
-    )
     started = []
 
     def ship(src, dst, send, recv, target):
@@ -504,6 +476,7 @@
         pass_on(normed, 0, tp, {"tp": p * INNER + c})
     pass_on(normed, 0, tp, {"tp": x * INNER + other})
     tokens[0, tp] = normed[...]
+    close()
 
     def spread(k):
         arrive(tokens.at[k, tp], r_tok.at[k, tp])
@@ -571,44 +544,79 @@
         copy.wait_send()
 
 
-def tail(normed, mid, up, down, total, lanes):
+def layer_kernel(outer, lanes, scales, *refs):
+    operands, out, carried = refs[:20], refs[20], refs[21:25]
+    close, started = front_kernel(outer, lanes, scales, *operands, *carried, *refs[25:35])
+    up_all, down_all, mid, normed = carried
+    sides = lanes // INNER
+    tail_kernel(outer, sides, close, normed, mid, up_all, down_all, out, *refs[35:])
+    for copy in started:
+        copy.wait_send()
+
+
+def layer(operands, total, lanes):
+    count = operands[0].shape[0]
+    q_a, q_b, resid = operands[4], operands[5], operands[14]
+    up, down = operands[18], operands[19]
     outer = total // INNER
     sides = lanes // INNER
-    rows, width = mid.shape
+    rows, width = resid.shape
+    units = up.shape[1] // outer
     kind = jnp.bfloat16
+    scales = ((LANES // 2) ** (-0.5), LANES ** (-0.5))
+    features = q_a.shape[1] + q_b.shape[1]
     vmem = pl.BlockSpec(memory_space=pltpu.VMEM)
     sems = pltpu.SemaphoreType.DMA
     moves = outer - 1 + outer * (2 * sides - 1)
     near = sides - 1
     far = outer - 1
+    carried = [
+        pltpu.VMEM((up.shape[0] * total, units), kind),
+        pltpu.VMEM((units, down.shape[1] * total), kind),
+        pltpu.VMEM(resid.shape, kind),
+        pltpu.VMEM(resid.shape, kind),
+    ]
+    first = [
+        pltpu.VMEM((count, 3 * LANES), kind),
+        pltpu.VMEM((total, count, 3 * LANES), kind),
+        pltpu.VMEM((count, features), kind),
+        pltpu.VMEM((lanes, rows, width), kind),
+        pltpu.VMEM((lanes, rows, width), kind),
+        sems((3, total)),
+        sems((3, total)),
+        sems((3,)),
+        sems((lanes - 1,)),
+        sems((lanes,)),
+    ]
+    second = [
+        pltpu.VMEM((outer, lanes, rows, width), kind),
+        pltpu.VMEM((outer, sides, rows, width), kind),
+        pltpu.VMEM((outer, sides, rows, width), kind),
+        pltpu.VMEM((outer, sides, rows, width), kind),
+        pltpu.VMEM((outer, near, rows, width), kind),
+        pltpu.VMEM((outer, rows, width), jnp.float32),
+        pltpu.VMEM((far, rows, width), kind),
+        pltpu.VMEM((far, rows, width), kind),
+        sems((moves,)),
+        sems((outer, lanes)),
+        sems((outer,)),
+        sems((outer,)),
+        sems((outer, near)),
+        sems((outer, near)),
+        sems((far,)),
+        sems((far,)),
+    ]
     return pl.pallas_call(
-        lambda *refs: tail_kernel(outer, sides, *refs),
-        out_shape=jax.ShapeDtypeStruct(mid.shape, mid.dtype),
-        in_specs=[vmem] * 4,
+        lambda *refs: layer_kernel(outer, lanes, scales, *refs),
+        out_shape=jax.ShapeDtypeStruct(resid.shape, resid.dtype),
+        in_specs=[vmem] * 20,
         out_specs=vmem,
-        scratch_shapes=[
-            pltpu.VMEM((outer, lanes, rows, width), kind),
-            pltpu.VMEM((outer, sides, rows, width), kind),
-            pltpu.VMEM((outer, sides, rows, width), kind),
-            pltpu.VMEM((outer, sides, rows, width), kind),
-            pltpu.VMEM((outer, near, rows, width), kind),
-            pltpu.VMEM((outer, rows, width), jnp.float32),
-            pltpu.VMEM((far, rows, width), kind),
-            pltpu.VMEM((far, rows, width), kind),
-            sems((moves,)),
-            sems((outer, lanes)),
-            sems((outer,)),
-            sems((outer,)),
-            sems((outer, near)),
-            sems((outer, near)),
-            sems((far,)),
-            sems((far,)),
-        ],
+        scratch_shapes=carried + first + second,
         compiler_params=pltpu.CompilerParams(
-            collective_id=1, has_side_effects=True, vmem_limit_bytes=56 * 1024 * 1024
+            collective_id=0, has_side_effects=True, vmem_limit_bytes=60 * 1024 * 1024
         ),
-        name="tail",
-    )(normed, mid, up, down)
+        name="layer",
+    )(*operands)
 
 
 def turning_table(places, width, repeat):
@@ -642,28 +650,12 @@
 ):
     count = query_a.shape[0]
     places = lax.axis_index("sp") * count + jnp.arange(count, dtype=jnp.int32)
-    kv = jnp.concatenate([key_b, value_b, key_a, value_a], axis=1)
-    table = jnp.concatenate(
-        turning_table(places, gain_qb.shape[0], 1) + turning_table(places, gain_qa.shape[0], 2),
-        axis=1,
-    )
-    gains = jnp.stack([gain_qb, gain_kb, jnp.tile(gain_qa, 2), jnp.tile(gain_ka, 2)])
-    up, down, mid, normed = front(
-        kv,
-        query_a,
-        query_b,
-        table,
-        gains,
-        resid,
-        norm_gain.reshape(1, -1),
-        w_out_a,
-        w_out_b,
-        w_up,
-        w_down,
-        total,
-        lanes,
-    )
-    return tail(normed, mid, up, down, total, lanes)
+    cos_a, sin_a = turning_table(places, gain_qa.shape[0], 2)
+    cos_b, sin_b = turning_table(places, gain_qb.shape[0], 1)
+    gains = [g.reshape(1, -1) for g in (gain_qa, gain_ka, gain_qb, gain_kb)]
+    operands = [key_a, value_a, key_b, value_b, query_a, query_b, cos_a, sin_a, cos_b, sin_b]
+    operands += gains + [resid, norm_gain.reshape(1, -1), w_out_a, w_out_b, w_up, w_down]
+    return layer(operands, total, lanes)
 
 
 def fits(total, lanes, args):

time: 174 us -> 148 us (0.85)
  Pallas kernels: 164 us -> 142 us
  other arithmetic: 4.79 us -> 1.84 us
    pallas_call x2 -> x1, Pallas kernels: 164 us -> 142 us  [layer(): pl.pallas_call(lambda *refs: layer_kernel(outer, lanes, scales, *refs), o...]
    concatenate x2 -> x0, other arithmetic: 2.5 us -> none  [the longest x1 1.65 us: kernel_local(): kv = jnp.concatenate([key_b, value_b, key_a, value_a], axis=1)]
    sin x0 -> x1, other arithmetic: none -> 1.81 us  [turning_table(): return [jnp.cos(angles), jnp.sin(angles)]]
    unnamed x3 -> x7, local copies, waits for them, and re-layouts: 3.42 us -> 3.87 us
where the time goes in v3:
time: 148 us
  Pallas kernels  142 us (96%)
  local copies, waits for them, and re-layouts  3.87 us (3%)
  other arithmetic  1.84 us (1%)
    pallas_call x1, Pallas kernels, layer(): pl.pallas_call(lambda *refs: layer_kernel(outer, lanes, scales, *refs), o...  142 us
    unnamed x7, local copies, waits for them, and re-layouts  3.87 us

profile of v3, /device:TPU:0, one launch (start us, length us, event | category | flops | bytes accessed | tf_op | source)
XLA Modules:
  0.0 148.1 jit_solution(6850154150248296690)
XLA Ops:
  0.0 0.0 copy-start
  0.0 0.7 copy-done
  0.8 0.0 copy-start.1
  0.8 0.7 copy.17.refs_0_
  1.5 0.0 copy-done.1
  1.5 0.7 copy.18.refs_1_
  2.2 1.8 %fusion = (f32[256,128]{1,0:T(8,128)}, f32[256,128]{1,0:T(8,128)}, f32[256,128]{1,0:T(8,128)}, f32[256,128]{1,0:T(8,128)}) fusion(f32[128]{0:T(128)S(1)} %get-tuple-element.14, s32[256]{0:T(256)S(1)} %get-tuple-element.11, s32[256]{0:T(256)S(1)} %get-tuple-element.12, pred[128]{0:T(512)(128)(4,1)S(1)} %get-tuple-element.16, f32[128]{0:T(128)S(1)} %get-tuple-element.13, ...), kind=kLoop, calls=%fused_computation.1 | loop fusion | flops 196608 | bytes 527616 | tf_op jit(solution)/shard_map/sin | solution.py:628
  4.0 142.3 %layer.1 = bf16[64,2048]{1,0:T(8,128)(2,1)} custom-call(bf16[256,64]{1,0:T(8,128)(2,1)} %copy.17.refs_0_, bf16[256,64]{1,0:T(8,128)(2,1)} %copy.18.refs_1_, bf16[256,128]{1,0:T(8,128)(2,1)} %refs_2_.1, bf16[256,128]{1,0:T(8,128)(2,1)} %refs_3_.1, bf16[256,256]{1,0:T(8,128)(2,1)} %refs_4_.1, bf16[256,256]{1,0:T(8,128)(2,1)} %refs_5_.1, ...), custom_call_target="tpu_custom_call" | custom-call | tf_op jit(solution)/shard_map/layer/pallas_call | solution.py:609
  146.4 1.7 %copy.20 = bf16[64,2048]{1,0:T(8,128)(2,1)} copy(bf16[64,2048]{1,0:T(8,128)(2,1)} %layer.1) | data formatting | bytes 524288
  (3 shorter events, 0.0 us)
Async XLA Ops:
  0.0 0.8 copy-start
  0.8 0.8 copy-start.1
